TPU v7x, 32 devices: a whole 2x2x4 slice. The times are simulated.
32 devices in a mesh: ra: 4 (over z), cb: 4 (over y, x), dp: 2 (over core).
Axes of the slice: x: 2, y: 2, z: 4, core: 2. Of those that a mesh axis runs over, the one named last changes fastest.
Arguments:
- tokens: bfloat16 [256, 2048], P('dp', 'ra'), may hold values from -200 to 200, as said below
- first_gain: float32 [2048], P('ra'), may hold values from 0.1 to 1.9
- first_gate: float32 [2048, 5632], P('ra', 'cb'), may hold values from -0.125 to 0.125
- first_gate_scale: float32 [5632], P('cb'), may hold values from 0.5 to 2
- first_up: float32 [2048, 5632], P('ra', 'cb'), may hold values from -0.125 to 0.125
- first_up_scale: float32 [5632], P('cb'), may hold values from 0.5 to 2
- first_down: float32 [5632, 2048], P('cb', 'ra'), may hold values from -0.078125 to 0.078125
- first_down_scale: float32 [2048], P('ra'), may hold values from 0.5 to 2
- second_gain: float32 [2048], P('ra'), may hold values from 0.1 to 1.9
- second_gate: float32 [2048, 5632], P('ra', 'cb'), may hold values from -0.125 to 0.125
- second_gate_scale: float32 [5632], P('cb'), may hold values from 0.5 to 2
- second_up: float32 [2048, 5632], P('ra', 'cb'), may hold values from -0.125 to 0.125
- second_up_scale: float32 [5632], P('cb'), may hold values from 0.5 to 2
- second_down: float32 [5632, 2048], P('cb', 'ra'), may hold values from -0.078125 to 0.078125
- second_down_scale: float32 [2048], P('ra'), may hold values from 0.5 to 2
Outputs:
- stream_out: bfloat16 [256, 2048], P('dp', 'ra')
Inputs may be any that keep to these rules, and one draw needn't show every extreme that they name: `tokens`: Per-token and per-feature magnitudes vary.
All inputs are finite; a program needn't handle non-finite values.
Results may differ from a plain program's by a relative error of at most 0.039.
Values may be sent and summed in bfloat16 or wider, within the bound.
A program may use at most 64 MiB of HBM per device.

v0:
```python
import jax
import jax.numpy as jnp
from jax import lax
from jax.sharding import PartitionSpec as P

D = 2048


EPS = 1e-06
RESID = 0.5


def sublayer(stream, gain, w_gate, gate_scale, w_up, up_scale, w_down, down_scale):
    values = stream.astype(jnp.float32)
    sum_sq = lax.psum(jnp.sum(values * values, -1), "ra")
    normed = (values * lax.rsqrt(sum_sq / D + EPS)[:, None] * gain).astype(jnp.bfloat16)
    part_gate = jnp.dot(normed, w_gate.astype(jnp.bfloat16), preferred_element_type=jnp.float32)
    part_up = jnp.dot(normed, w_up.astype(jnp.bfloat16), preferred_element_type=jnp.float32)
    gate, up = (
        lax.psum(part_gate.astype(jnp.bfloat16), "ra").astype(jnp.float32),
        lax.psum(part_up.astype(jnp.bfloat16), "ra").astype(jnp.float32),
    )
    hidden = (jax.nn.silu(gate * gate_scale) * (up * up_scale)).astype(jnp.bfloat16)
    partial_value = jnp.dot(hidden, w_down.astype(jnp.bfloat16), preferred_element_type=jnp.float32)
    branch = lax.psum(partial_value.astype(jnp.bfloat16), "cb").astype(jnp.float32)
    return (RESID * values + branch * down_scale).astype(jnp.bfloat16)


def body(
    tokens,
    first_gain,
    first_gate,
    first_gate_scale,
    first_up,
    first_up_scale,
    first_down,
    first_down_scale,
    second_gain,
    second_gate,
    second_gate_scale,
    second_up,
    second_up_scale,
    second_down,
    second_down_scale,
):
    middle = sublayer(
        tokens,
        first_gain,
        first_gate,
        first_gate_scale,
        first_up,
        first_up_scale,
        first_down,
        first_down_scale,
    )
    return sublayer(
        middle,
        second_gain,
        second_gate,
        second_gate_scale,
        second_up,
        second_up_scale,
        second_down,
        second_down_scale,
    )


def solution(mesh):
    in_specs = (
        P("dp", "ra"),
        P("ra"),
        P("ra", "cb"),
        P("cb"),
        P("ra", "cb"),
        P("cb"),
        P("cb", "ra"),
        P("ra"),
        P("ra"),
        P("ra", "cb"),
        P("cb"),
        P("ra", "cb"),
        P("cb"),
        P("cb", "ra"),
        P("ra"),
    )
    out_specs = P("dp", "ra")
    return jax.shard_map(body, mesh=mesh, in_specs=in_specs, out_specs=out_specs, check_vma=False)
```

profile of v0, /device:TPU:0, one launch (start us, length us, event | category | flops | bytes accessed | tf_op | source)
XLA Modules:
  0.0 218.9 jit_solution(4206691932930138170)
XLA Ops:
  6.5 0.0 all-reduce.13.cloned.1.call-start
  6.5 1.2 fusion.22
  7.7 13.5 %psum.56 = f32[128]{0:T(128)S(1)} all-reduce(f32[128]{0:T(128)S(1)} %fusion.22), channel_id=1, replica_groups=mesh['ra'=4,'cb'=4,'dp'=2] {'ra'}, use_global_device_ids=true, to_apply=%region_1.0 | all-reduce | flops 128 | bytes 1024 | tf_op jit(solution)/shard_map/psum | solution.py:15
  21.2 3.1 %convolution_convert_fusion.2 = bf16[128,1408]{1,0:T(8,128)(2,1)} fusion(f32[512,1408]{1,0:T(8,128)} %param.19, bf16[128,512]{1,0:T(8,128)(2,1)} %param.15, f32[512]{0:T(512)} %param.16, f32[128]{0:T(128)S(1)} %add_rsqrt_fusion.1), kind=kOutput, calls=%fused_computation.2 | convolution fusion | flops 185712640 | bytes 3377664 | tf_op jit(solution)/shard_map/dot_general | solution.py:18
  24.3 0.0 copy-done.3
  24.3 0.0 copy-done.4
  24.3 0.0 copy-done
  24.3 0.0 copy-start.9
  24.3 0.0 copy-start.10
  24.3 1.2 convolution_convert_fusion.3
  25.5 0.0 all-reduce.13.cloned.1.call-update
  25.5 0.0 all-reduce.7.cloned.1.call-start
  25.6 40.3 %all-reduce.13.cloned.1.call-done = (bf16[128,1408]{1,0:T(8,128)(2,1)}, bf16[128,1408]{1,0:T(8,128)(2,1)}) async-done(((bf16[128,1408]{1,0:T(8,128)(2,1)}, bf16[128,1408]{1,0:T(8,128)(2,1)}), (bf16[128,1408]{1,0:T(8,128)(2,1)}, bf16[128,1408]{1,0:T(8,128)(2,1)})) %all-reduce.13.cloned.1.call-update) | async-done | bytes 720912 | tf_op jit(solution)/shard_map/psum | solution.py:21
  65.9 3.2 %fusion.8 = bf16[128,512]{1,0:T(8,128)(2,1)} fusion(f32[1408,512]{1,0:T(8,128)} %param.21, bf16[128,1408]{1,0:T(8,128)(2,1)} %get-tuple-element.7, bf16[128,1408]{1,0:T(8,128)(2,1)} %get-tuple-element.8, f32[1408]{0:T(1024)S(1)} %copy-done.9, f32[1408]{0:T(1024)S(1)} %copy-done.10), kind=kOutput, calls=%fused_computation.12 | convolution fusion | flops 187138048 | bytes 3746816 | tf_op jit(solution)/shard_map/dot_general | solution.py:24
  69.1 0.0 all-reduce.7.cloned.1.call-update
  69.1 0.0 all-reduce.11.cloned.1.call-start
  69.1 41.8 %all-reduce.7.cloned.1.call-done = bf16[128,512]{1,0:T(8,128)(2,1)} async-done(((bf16[128,512]{1,0:T(8,128)(2,1)}), bf16[128,512]{1,0:T(8,128)(2,1)}) %all-reduce.7.cloned.1.call-update) | async-done | bytes 131088 | tf_op jit(solution)/shard_map/psum | solution.py:25
  111.0 0.0 copy-done.6
  111.0 1.0 fusion.27
  112.0 11.7 %psum.60 = f32[128]{0:T(128)S(1)} all-reduce(f32[128]{0:T(128)S(1)} %get-tuple-element.9), channel_id=1, replica_groups=mesh['ra'=4,'cb'=4,'dp'=2] {'ra'}, use_global_device_ids=true, to_apply=%region_6.7 | all-reduce | flops 128 | bytes 1024 | tf_op jit(solution)/shard_map/psum | solution.py:15
  123.7 1.2 convolution_convert_fusion
  124.9 0.8 copy-done.2
  125.7 1.2 convolution_convert_fusion.1
  126.8 0.0 all-reduce.11.cloned.1.call-update
  126.9 0.0 all-reduce.9.cloned.1.call-start
  126.9 39.3 %all-reduce.11.cloned.1.call-done = (bf16[128,1408]{1,0:T(8,128)(2,1)}, bf16[128,1408]{1,0:T(8,128)(2,1)}) async-done(((bf16[128,1408]{1,0:T(8,128)(2,1)}, bf16[128,1408]{1,0:T(8,128)(2,1)}), (bf16[128,1408]{1,0:T(8,128)(2,1)}, bf16[128,1408]{1,0:T(8,128)(2,1)})) %all-reduce.11.cloned.1.call-update) | async-done | bytes 720912 | tf_op jit(solution)/shard_map/psum | solution.py:21
  166.3 0.0 copy-done.8
  166.3 0.0 copy-done.12
  166.3 2.3 %fusion.11 = bf16[128,512]{1,0:T(8,128)(2,1)} fusion(f32[1408,512]{1,0:T(8,128)S(1)} %copy-done.8, bf16[128,1408]{1,0:T(8,128)(2,1)} %get-tuple-element.5, bf16[128,1408]{1,0:T(8,128)(2,1)} %get-tuple-element.6, f32[1408]{0:T(1024)S(1)} %copy-done.11, f32[1408]{0:T(1024)S(1)} %copy-done.12), kind=kOutput, calls=%fused_computation.13 | convolution fusion | flops 187138048 | bytes 3746816 | tf_op jit(solution)/shard_map/dot_general | solution.py:24
  168.5 0.0 all-reduce.9.cloned.1.call-update
  168.6 42.2 %all-reduce.9.cloned.1.call-done = bf16[128,512]{1,0:T(8,128)(2,1)} async-done(((bf16[128,512]{1,0:T(8,128)(2,1)}), bf16[128,512]{1,0:T(8,128)(2,1)}) %all-reduce.9.cloned.1.call-update) | async-done | bytes 131088 | tf_op jit(solution)/shard_map/psum | solution.py:25
  210.8 1.6 fusion.26
  (19 shorter events, 0.0 us)
Async XLA Ops:
  6.5 17.7 %copy-start.3 = (bf16[128,512]{1,0:T(8,128)(2,1)S(1)}, bf16[128,512]{1,0:T(8,128)(2,1)}, u32[]{:S(2)}) copy-start(bf16[128,512]{1,0:T(8,128)(2,1)} %param.15) | copy-start | bytes 393220
  6.5 17.7 %copy-start.4 = (f32[512]{0:T(512)S(1)}, f32[512]{0:T(512)}, u32[]{:S(2)}) copy-start(f32[512]{0:T(512)} %param.16) | copy-start | bytes 6148
  6.5 17.7 %copy-start = (f32[512,1408]{1,0:T(8,128)S(1)}, f32[512,1408]{1,0:T(8,128)}, u32[]{:S(2)}) copy-start(f32[512,1408]{1,0:T(8,128)} %param.17) | copy-start | bytes 8650756
  6.5 59.3 %all-reduce.13.cloned.1.call-start = ((), (), s32[]{:S(2)}) async-start(), calls=%async_computation.3 | async-start | bytes 1441792 | tf_op jit(solution)/shard_map/psum | solution.py:21
  24.3 41.6 %copy-start.9 = (f32[1408]{0:T(1024)S(1)}, f32[1408]{0:T(1024)}, u32[]{:S(2)}) copy-start(f32[1408]{0:T(1024)} %param.20) | copy-start | bytes 16900
  24.3 41.6 %copy-start.10 = (f32[1408]{0:T(1024)S(1)}, f32[1408]{0:T(1024)}, u32[]{:S(2)}) copy-start(f32[1408]{0:T(1024)} %param.18) | copy-start | bytes 16900
  25.5 85.5 %copy-start.6 = (f32[512]{0:T(512)S(1)}, f32[512]{0:T(512)}, u32[]{:S(2)}) copy-start(f32[512]{0:T(512)} %param.22) | copy-start | bytes 6148
  25.5 98.2 %copy-start.1 = (f32[512,1408]{1,0:T(8,128)S(1)}, f32[512,1408]{1,0:T(8,128)}, u32[]{:S(2)}) copy-start(f32[512,1408]{1,0:T(8,128)} %param.26) | copy-start | bytes 8650756
  25.5 98.2 %copy-start.5 = (f32[512]{0:T(512)S(1)}, f32[512]{0:T(512)}, u32[]{:S(2)}) copy-start(f32[512]{0:T(512)} %param.23) | copy-start | bytes 6148
  25.5 85.5 %all-reduce.7.cloned.1.call-start = ((), (), s32[]{:S(2)}) async-start(), calls=%async_computation | async-start | bytes 262144 | tf_op jit(solution)/shard_map/psum | solution.py:25
  69.1 97.2 %all-reduce.11.cloned.1.call-start = ((), (), s32[]{:S(2)}) async-start(), calls=%async_computation.2 | async-start | bytes 1441792 | tf_op jit(solution)/shard_map/psum | solution.py:21
  123.7 1.9 copy-start.2
  125.7 40.6 %copy-start.8 = (f32[1408,512]{1,0:T(8,128)S(1)}, f32[1408,512]{1,0:T(8,128)}, u32[]{:S(2)}) copy-start(f32[1408,512]{1,0:T(8,128)} %param.28) | copy-start | bytes 8650756
  125.7 40.6 %copy-start.11 = (f32[1408]{0:T(1024)S(1)}, f32[1408]{0:T(1024)}, u32[]{:S(2)}) copy-start(f32[1408]{0:T(1024)} %param.27) | copy-start | bytes 16900
  125.7 40.6 %copy-start.12 = (f32[1408]{0:T(1024)S(1)}, f32[1408]{0:T(1024)}, u32[]{:S(2)}) copy-start(f32[1408]{0:T(1024)} %param.25) | copy-start | bytes 16900
  126.8 83.9 %copy-start.7 = (f32[512]{0:T(512)S(1)}, f32[512]{0:T(512)}, u32[]{:S(2)}) copy-start(f32[512]{0:T(512)} %param.29) | copy-start | bytes 6148
  126.9 83.9 %all-reduce.9.cloned.1.call-start = ((), (), s32[]{:S(2)}) async-start(), calls=%async_computation.1 | async-start | bytes 262144 | tf_op jit(solution)/shard_map/psum | solution.py:25
Sparse Core Ops, SparseCore 0:
  25.6 40.1 all-reduce.12
  69.2 41.7 all-reduce.6
  127.0 39.2 all-reduce.10
  169.0 41.7 all-reduce.8
where the time goes:
time: 219 us
  waiting for transfers between devices  164 us (75%)
  blocking collectives  25.2 us (12%)
  between operations  13.2 us (6%)
  matrix products  12 us (5%)
  other arithmetic  3.83 us (2%)
    psum x2, waiting for transfers between devices, sublayer(): lax.psum(partial_value.astype(jnp.bfloat16), 'cb').astype(jnp.float32)  84 us
    psum x2, waiting for transfers between devices, sublayer(): lax.psum(part_up.astype(jnp.bfloat16), 'ra').astype(jnp.float32)  79.7 us
    psum x2, blocking collectives, sublayer(): sum_sq = lax.psum(jnp.sum(values * values, -1), 'ra')  25.2 us
    dot_general x2, matrix products, sublayer(): jnp.dot(hidden, w_down.astype(jnp.bfloat16), preferred_element_type=jnp.f...  5.45 us
  transfers between devices with their start and end apart: 4, of which 4 were waited for; matrix products, arithmetic and copies ran while one was open for 0% of the time, Pallas kernels for 0%

commit v1 on v0

v1 whole, which is shorter than its diff:
```python
import functools

import jax
import jax.numpy as jnp
from jax import lax
from jax.experimental import pallas as pl
from jax.experimental.pallas import tpu as pltpu
from jax.sharding import PartitionSpec as P

EPS = 1e-06
RESID = 0.5
MESH = pl.DeviceIdType.MESH
CHUNK = 128
LAG = 3
PIECES = 2


def kernel(
    n_ra, n_cb, width,
    tokens, gain1, gs1, us1, ds1, gain2, gs2, us2, ds2,
    wg1, wu1, wd1, wg2, wu2, wd2,
    out,
    wg, wu, wd, part, rs_send, rs_recv, hid, ss_send, ss_recv, inv, xs, stream, cb_send, cb_recv,
    wg_sem, wu_sem, wd_sem,
    rs_ss, rs_rs, ag_ss, ag_rs, sq_ss, sq_rs, cb_ss, cb_rs,
):
    p = lax.axis_index("ra")
    c = lax.axis_index("cb")
    tok = tokens.shape[0]
    half = tok // 2
    chunks = wg.shape[2] // CHUNK
    last = n_ra - 1
    phases = n_cb.bit_length() - 1
    rows_of = half // PIECES
    gates, ups, downs = (wg1, wg2), (wu1, wu2), (wd1, wd2)

    def cols(k):
        return pl.ds(pl.multiple_of(k * CHUNK, CHUNK), CHUNK)

    def load_pair(layer, k):
        return (
            pltpu.make_async_copy(gates[layer].at[:, cols(k)], wg.at[layer, :, cols(k)], wg_sem.at[layer, k]),
            pltpu.make_async_copy(ups[layer].at[:, cols(k)], wu.at[layer, :, cols(k)], wu_sem.at[layer, k]),
        )

    def load_down(layer):
        return pltpu.make_async_copy(downs[layer], wd.at[layer], wd_sem.at[layer])

    def start_pairs(layer):
        @pl.loop(0, chunks)
        def _(k):
            for copy in load_pair(layer, k):
                copy.start()

    start_pairs(0)
    load_down(0).start()

    def partner(bit):
        return c + bit - 2 * bit * ((c // bit) % 2)

    barrier = pltpu.get_barrier_semaphore()

    @pl.when(p > 0)
    def _():
        pl.semaphore_signal(barrier, inc=1, device_id={"ra": p - 1}, device_id_type=MESH)

    @pl.when(p < last)
    def _():
        pl.semaphore_signal(barrier, inc=1, device_id={"ra": p + 1}, device_id_type=MESH)

    for b in range(phases):
        pl.semaphore_signal(barrier, inc=1, device_id={"cb": partner(1 << b)}, device_id_type=MESH)

    def place(way):
        return (p, p + 1, p - 1) if way == 0 else (last - p, p - 1, p + 1)

    def rs_copy(layer, way, k, to):
        return pltpu.make_async_remote_copy(
            src_ref=rs_send.at[layer, way, k], dst_ref=rs_recv.at[layer, way, k],
            send_sem=rs_ss.at[layer, way, k], recv_sem=rs_rs.at[layer, way, k],
            device_id={"ra": to}, device_id_type=MESH)

    def sq_copy(layer, way, to):
        return pltpu.make_async_remote_copy(
            src_ref=ss_send.at[layer, way], dst_ref=ss_recv.at[layer, way],
            send_sem=sq_ss.at[layer, way], recv_sem=sq_rs.at[layer, way],
            device_id={"ra": to}, device_id_type=MESH)

    def ag_copy(layer, way, k, to):
        piece = hid.at[layer, pl.ds(way * half, half), cols(k)]
        return pltpu.make_async_remote_copy(
            src_ref=piece, dst_ref=piece,
            send_sem=ag_ss.at[layer, way, k], recv_sem=ag_rs.at[layer, way, k],
            device_id={"ra": to}, device_id_type=MESH)

    def cb_copy(layer, phase, h, g):
        bit = 1 << ((phase + h) % phases)
        return pltpu.make_async_remote_copy(
            src_ref=cb_send.at[layer, phase, h, g], dst_ref=cb_recv.at[layer, phase, h, g],
            send_sem=cb_ss.at[layer, phase, h, g], recv_sem=cb_rs.at[layer, phase, h, g],
            device_id={"cb": partner(bit)}, device_id_type=MESH)

    for layer in range(2):
        gain = (gain1, gain2)[layer]
        gscale, uscale, dscale = (gs1, gs2)[layer], (us1, us2)[layer], (ds1, ds2)[layer]
        values = (tokens if layer == 0 else stream)[...].astype(jnp.float32)
        xs[...] = (values * gain[...]).astype(jnp.bfloat16)
        sums = jnp.sum(values * values, axis=-1, keepdims=True)
        flat = jnp.broadcast_to(sums, (tok, 128)).T[:8]
        ss_send[layer, 0] = flat
        ss_send[layer, 1] = flat
        if layer == 0:
            pl.semaphore_wait(barrier, (p > 0).astype(jnp.int32) + (p < last).astype(jnp.int32) + phases)
        for way in range(2):
            at, ahead, _ = place(way)

            @pl.when(at == 0)
            def _():
                sq_copy(layer, way, ahead).start()

        @pl.loop(0, chunks + LAG * 2 * last)
        def _(t):
            @pl.when(t < chunks)
            def _():
                for copy in load_pair(layer, t):
                    copy.wait()
                w = jnp.concatenate(
                    [wg[layer, :, cols(t)].astype(jnp.bfloat16), wu[layer, :, cols(t)].astype(jnp.bfloat16)], axis=1)
                prod = jnp.dot(xs[...], w, preferred_element_type=jnp.float32)
                part[t] = prod
                for way in range(2):
                    at, ahead, _ = place(way)

                    @pl.when(at == 0)
                    def _():
                        rs_send[layer, way, t] = prod[way * half:(way + 1) * half].astype(jnp.bfloat16)
                        rs_copy(layer, way, t, ahead).start()

            for way in range(2):
                at, ahead, behind = place(way)
                lo = way * half
                k = t - LAG * at
                inside = (k >= 0) & (k < chunks) & (at > 0)

                @pl.when(inside & (k == 0))
                def _():
                    sq_copy(layer, way, ahead).wait_recv()
                    total = ss_recv[layer, way] + ss_send[layer, way]

                    @pl.when(at < last)
                    def _():
                        ss_send[layer, way] = total
                        sq_copy(layer, way, ahead).start()

                    @pl.when(at == last)
                    def _():
                        column = jnp.broadcast_to(total[:1], (128, tok)).T
                        inv[way] = lax.rsqrt(column[lo:lo + half] / width + EPS)

                @pl.when(inside)
                def _():
                    rs_copy(layer, way, k, ahead).wait_recv()
                    total = rs_recv[layer, way, k].astype(jnp.float32) + part[k, lo:lo + half, :]

                    @pl.when(at < last)
                    def _():
                        rs_send[layer, way, k] = total.astype(jnp.bfloat16)
                        rs_copy(layer, way, k, ahead).start()

                    @pl.when(at == last)
                    def _():
                        scale = inv[way]
                        gate = total[:, :CHUNK] * scale * gscale[:, cols(k)]
                        up = total[:, CHUNK:] * scale * uscale[:, cols(k)]
                        hidden = gate / (1.0 + jnp.exp(-gate)) * up
                        hid[layer, lo:lo + half, cols(k)] = hidden.astype(jnp.bfloat16)
                        ag_copy(layer, way, k, behind).start()

                j = t - LAG * (2 * last - at)

                @pl.when((j >= 0) & (j < chunks) & (at < last))
                def _():
                    ag_copy(layer, way, j, behind).wait_recv()

                    @pl.when(at > 0)
                    def _():
                        ag_copy(layer, way, j, behind).start()

            if layer == 0:
                @pl.when(t == chunks)
                def _():
                    start_pairs(1)
                    load_down(1).start()

        load_down(layer).wait()
        down = jnp.dot(hid[layer], wd[layer].astype(jnp.bfloat16), preferred_element_type=jnp.float32)
        order = [(h, g) for g in range(PIECES) for h in range(2)]
        for h, g in order:
            lo = h * half + g * rows_of
            cb_send[layer, 0, h, g] = down[lo:lo + rows_of].astype(jnp.bfloat16)
            cb_copy(layer, 0, h, g).start()
        for phase in range(phases):
            for h, g in order:
                cb_copy(layer, phase, h, g).wait_recv()
                total = cb_send[layer, phase, h, g].astype(jnp.float32) + cb_recv[layer, phase, h, g].astype(jnp.float32)
                if phase < phases - 1:
                    cb_send[layer, phase + 1, h, g] = total.astype(jnp.bfloat16)
                    cb_copy(layer, phase + 1, h, g).start()
                else:
                    lo = h * half + g * rows_of
                    old = (tokens if layer == 0 else stream)[lo:lo + rows_of, :].astype(jnp.float32)
                    new = (RESID * old + total * dscale[...]).astype(jnp.bfloat16)
                    if layer == 0:
                        stream[lo:lo + rows_of, :] = new
                    else:
                        out[lo:lo + rows_of, :] = new

    for layer in range(2):
        for way in range(2):
            at, ahead, behind = place(way)

            @pl.when(at < last)
            def _():
                sq_copy(layer, way, ahead).wait_send()

                @pl.loop(0, chunks)
                def _(k):
                    rs_copy(layer, way, k, ahead).wait_send()

            @pl.when(at > 0)
            def _():
                @pl.loop(0, chunks)
                def _(k):
                    ag_copy(layer, way, k, behind).wait_send()

        for phase in range(phases):
            for h in range(2):
                for g in range(PIECES):
                    cb_copy(layer, phase, h, g).wait_send()


def solution(mesh):
    n_ra, n_cb = mesh.shape["ra"], mesh.shape["cb"]
    names = ("tokens", "g1", "wg1", "gs1", "wu1", "us1", "wd1", "ds1", "g2", "wg2", "gs2", "wu2", "us2", "wd2", "ds2")

    def body(*args):
        a = dict(zip(names, args))
        small = [a[k].reshape(1, -1) for k in ("g1", "gs1", "us1", "ds1", "g2", "gs2", "us2", "ds2")]
        big = [a[k] for k in ("wg1", "wu1", "wd1", "wg2", "wu2", "wd2")]
        tok, dim = a["tokens"].shape
        ff = a["wg1"].shape[1]
        chunks, half, phases = ff // CHUNK, tok // 2, n_cb.bit_length() - 1
        f32, bf16, dma = jnp.float32, jnp.bfloat16, pltpu.SemaphoreType.DMA
        vmem = pl.BlockSpec(memory_space=pltpu.VMEM)
        piece = (2, phases, 2, PIECES)
        return pl.pallas_call(
            functools.partial(kernel, n_ra, n_cb, dim * n_ra),
            out_shape=jax.ShapeDtypeStruct((tok, dim), bf16),
            in_specs=[vmem] * 9 + [pl.BlockSpec(memory_space=pl.ANY)] * 6,
            out_specs=vmem,
            scratch_shapes=[
                pltpu.VMEM((2, dim, ff), f32), pltpu.VMEM((2, dim, ff), f32), pltpu.VMEM((2, ff, dim), f32),
                pltpu.VMEM((chunks, tok, 2 * CHUNK), f32),
                pltpu.VMEM((2, 2, chunks, half, 2 * CHUNK), bf16),
                pltpu.VMEM((2, 2, chunks, half, 2 * CHUNK), bf16),
                pltpu.VMEM((2, tok, ff), bf16),
                pltpu.VMEM((2, 2, 8, tok), f32), pltpu.VMEM((2, 2, 8, tok), f32),
                pltpu.VMEM((2, half, 128), f32),
                pltpu.VMEM((tok, dim), bf16), pltpu.VMEM((tok, dim), bf16),
                pltpu.VMEM(piece + (half // PIECES, dim), bf16), pltpu.VMEM(piece + (half // PIECES, dim), bf16),
                dma((2, chunks)), dma((2, chunks)), dma((2,)),
                dma((2, 2, chunks)), dma((2, 2, chunks)), dma((2, 2, chunks)), dma((2, 2, chunks)),
                dma((2, 2)), dma((2, 2)), dma(piece), dma(piece),
            ],
            compiler_params=pltpu.CompilerParams(
                collective_id=0, has_side_effects=True, vmem_limit_bytes=56 * 1024 * 1024),
        )(a["tokens"], *small, *big)

    in_specs = (
        P("dp", "ra"),
        P("ra"), P("ra", "cb"), P("cb"), P("ra", "cb"), P("cb"), P("cb", "ra"), P("ra"),
        P("ra"), P("ra", "cb"), P("cb"), P("ra", "cb"), P("cb"), P("cb", "ra"), P("ra"),
    )
    return jax.shard_map(body, mesh=mesh, in_specs=in_specs, out_specs=P("dp", "ra"), check_vma=False)
```

time: 219 us -> 83.1 us (0.38)
  waiting for transfers between devices: 164 us -> 0 us
  Pallas kernels: 0 us -> 76 us
  blocking collectives: 25.2 us -> 0 us
  between operations: 13.2 us -> 0.01 us
  matrix products: 12 us -> 0 us
  local copies, waits for them, and re-layouts: 0.81 us -> 6.73 us
  other arithmetic: 3.83 us -> 0 us
    psum x4 -> x0, waiting for transfers between devices: 164 us -> none  [the longest x2 84 us: sublayer(): lax.psum(partial_value.astype(jnp.bfloat16), 'cb').astype(jnp.float32)]
    pallas_call x0 -> x1, Pallas kernels: none -> 76 us  [body(): pl.pallas_call(functools.partial(kernel, n_ra, n_cb, dim * n_ra), out_sha...]
    psum x2 -> x0, blocking collectives: 25.2 us -> none  [sublayer(): sum_sq = lax.psum(jnp.sum(values * values, -1), 'ra')]
    dot_general x6 -> x0, matrix products: 12 us -> none  [the longest x2 5.45 us: sublayer(): jnp.dot(hidden, w_down.astype(jnp.bfloat16), preferred_element_type=jnp.f...]
    reshape x0 -> x4, local copies, waits for them, and re-layouts: none -> 5.16 us  [body(): a[k].reshape(1, -1)]
    reduce_sum x2 -> x0, other arithmetic: 2.21 us -> none  [sublayer(): sum_sq = lax.psum(jnp.sum(values * values, -1), 'ra')]
  transfers between devices with their start and end apart: 4 -> 0, of which waited for: 4 -> 0; matrix products, arithmetic and copies ran while one was open for 0% -> 0% of each run, Pallas kernels for 0% -> 0%
where the time goes in v1:
time: 83.1 us; the launch traced here: 82.7 us
  Pallas kernels  76 us (91%)
  local copies, waits for them, and re-layouts  6.73 us (8%)
    pallas_call x1, Pallas kernels, body(): pl.pallas_call(functools.partial(kernel, n_ra, n_cb, dim * n_ra), out_sha...  76 us
    reshape x4, local copies, waits for them, and re-layouts, body(): a[k].reshape(1, -1)  5.16 us

profile of v1, /device:TPU:0, one launch (start us, length us, event | category | flops | bytes accessed | tf_op | source)
XLA Modules:
  0.0 82.7 jit_solution(14728192452544109166)
XLA Ops:
  0.0 1.3 %reshape.25.gs1 = f32[1,1408]{1,0:T(1,128)} reshape(f32[1408]{0:T(1024)} %param.18) | data formatting | bytes 11264 | tf_op jit(solution)/shard_map/reshape | solution.py:248
  1.3 1.3 %reshape.26.us1 = f32[1,1408]{1,0:T(1,128)} reshape(f32[1408]{0:T(1024)} %param.20) | data formatting | bytes 11264 | tf_op jit(solution)/shard_map/reshape | solution.py:248
  2.6 1.3 %reshape.29.gs2 = f32[1,1408]{1,0:T(1,128)} reshape(f32[1408]{0:T(1024)} %param.25) | data formatting | bytes 11264 | tf_op jit(solution)/shard_map/reshape | solution.py:248
  3.9 1.3 %reshape.30.us2 = f32[1,1408]{1,0:T(1,128)} reshape(f32[1408]{0:T(1024)} %param.27) | data formatting | bytes 11264 | tf_op jit(solution)/shard_map/reshape | solution.py:248
  5.2 76.0 %shard_map.145 = bf16[128,512]{1,0:T(8,128)(2,1)} custom-call(bf16[128,512]{1,0:T(8,128)(2,1)} %tokens.1, f32[1,512]{1,0:T(1,128)} %bitcast.4, f32[1,1408]{1,0:T(1,128)} %reshape.25.gs1, f32[1,1408]{1,0:T(1,128)} %reshape.26.us1, f32[1,512]{1,0:T(1,128)} %bitcast.5, f32[1,512]{1,0:T(1,128)} %bitcast.6, f32[1,1408]{1,0:T(1,128)} %reshape.29.gs2, ...), custom_call_target="tpu_custom_call" | custom-call | tf_op jit(solution)/shard_map/pallas_call | solution.py:256
  81.1 1.6 %copy.17 = bf16[128,512]{1,0:T(8,128)(2,1)} copy(bf16[128,512]{1,0:T(8,128)(2,1)} %shard_map.145) | data formatting | bytes 262144

commit v2 on v1

v2 whole, which is shorter than its diff:
```python
import functools

import jax
import jax.numpy as jnp
from jax import lax
from jax.experimental import pallas as pl
from jax.experimental.pallas import tpu as pltpu
from jax.sharding import PartitionSpec as P

EPS = 1e-06
RESID = 0.5
MESH = pl.DeviceIdType.MESH
CHUNK = 128
LAG = 5
PIECES = 2


def kernel(
    n_ra, n_cb, width,
    tokens_in, gain1_in, gs1_in, us1_in, ds1_in, gain2_in, gs2_in, us2_in, ds2_in,
    wg1, wu1, wd1, wg2, wu2, wd2,
    out,
    tokens, gain1, gs1, us1, ds1, gain2, gs2, us2, ds2,
    wg, wu, wd, part, rs_send, rs_recv, hid, ss_send, ss_recv, inv, xs, stream, cb_send, cb_recv,
    in_sem, wg_sem, wu_sem, wd_sem,
    rs_ss, rs_rs, ag_ss, ag_rs, sq_ss, sq_rs, cb_ss, cb_rs,
):
    p = lax.axis_index("ra")
    c = lax.axis_index("cb")
    tok = tokens.shape[0]
    half = tok // 2
    chunks = wg.shape[2] // CHUNK
    last = n_ra - 1
    phases = n_cb.bit_length() - 1
    rows_of = half // PIECES
    gates, ups, downs = (wg1, wg2), (wu1, wu2), (wd1, wd2)

    def cols(k):
        return pl.ds(pl.multiple_of(k * CHUNK, CHUNK), CHUNK)

    def load_pair(layer, k):
        return (
            pltpu.make_async_copy(gates[layer].at[:, cols(k)], wg.at[layer, :, cols(k)], wg_sem.at[layer, k]),
            pltpu.make_async_copy(ups[layer].at[:, cols(k)], wu.at[layer, :, cols(k)], wu_sem.at[layer, k]),
        )

    def load_down(layer):
        return pltpu.make_async_copy(downs[layer], wd.at[layer], wd_sem.at[layer])

    def start_pairs(layer):
        @pl.loop(0, chunks)
        def _(k):
            for copy in load_pair(layer, k):
                copy.start()

    small = [
        pltpu.make_async_copy(a, b, in_sem.at[i])
        for i, (a, b) in enumerate((
            (tokens_in, tokens), (gain1_in, gain1), (gs1_in, gs1), (us1_in, us1), (ds1_in, ds1),
            (gain2_in, gain2), (gs2_in, gs2), (us2_in, us2), (ds2_in, ds2)))
    ]
    for copy in small:
        copy.start()
    start_pairs(0)
    load_down(0).start()

    def partner(bit):
        return c + bit - 2 * bit * ((c // bit) % 2)

    barrier = pltpu.get_barrier_semaphore()

    @pl.when(p > 0)
    def _():
        pl.semaphore_signal(barrier, inc=1, device_id={"ra": p - 1}, device_id_type=MESH)

    @pl.when(p < last)
    def _():
        pl.semaphore_signal(barrier, inc=1, device_id={"ra": p + 1}, device_id_type=MESH)

    for b in range(phases):
        pl.semaphore_signal(barrier, inc=1, device_id={"cb": partner(1 << b)}, device_id_type=MESH)

    mid = n_ra // 2
    delay = chunks
    final = max(LAG * mid, delay + LAG * (last - mid)) if last > mid else LAG * mid
    sides = range(2 if last > mid else 1)

    def place(way):
        return (p, p + 1, p - 1) if way == 0 else (last - p, p - 1, p + 1)

    def role(way):
        at, ahead, behind = place(way)
        side = (at > mid).astype(jnp.int32)
        hops = at + side * (last - 2 * at)
        inward = ahead + side * (behind - ahead)
        return at, side, hops, inward, ahead + behind - inward

    def rs_copy(layer, way, side, k, to):
        return pltpu.make_async_remote_copy(
            src_ref=rs_send.at[layer, way, k], dst_ref=rs_recv.at[layer, way, side, k],
            send_sem=rs_ss.at[layer, way, k], recv_sem=rs_rs.at[layer, way, side, k],
            device_id={"ra": to}, device_id_type=MESH)

    def sq_copy(layer, way, side, to):
        return pltpu.make_async_remote_copy(
            src_ref=ss_send.at[layer, way], dst_ref=ss_recv.at[layer, way, side],
            send_sem=sq_ss.at[layer, way], recv_sem=sq_rs.at[layer, way, side],
            device_id={"ra": to}, device_id_type=MESH)

    def ag_copy(layer, way, side, k, to):
        piece = hid.at[layer, pl.ds(way * half, half), cols(k)]
        return pltpu.make_async_remote_copy(
            src_ref=piece, dst_ref=piece,
            send_sem=ag_ss.at[layer, way, side, k], recv_sem=ag_rs.at[layer, way, k],
            device_id={"ra": to}, device_id_type=MESH)

    def cb_copy(layer, phase, h, g):
        bit = 1 << ((phase + h) % phases)
        return pltpu.make_async_remote_copy(
            src_ref=cb_send.at[layer, phase, h, g], dst_ref=cb_recv.at[layer, phase, h, g],
            send_sem=cb_ss.at[layer, phase, h, g], recv_sem=cb_rs.at[layer, phase, h, g],
            device_id={"cb": partner(bit)}, device_id_type=MESH)

    for copy in small:
        copy.wait()
    for layer in range(2):
        gain = (gain1, gain2)[layer]
        gscale, uscale, dscale = (gs1, gs2)[layer], (us1, us2)[layer], (ds1, ds2)[layer]
        values = (tokens if layer == 0 else stream)[...].astype(jnp.float32)
        xs[...] = (values * gain[...][None, :]).astype(jnp.bfloat16)
        sums = jnp.sum(values * values, axis=-1, keepdims=True)
        flat = jnp.broadcast_to(sums, (tok, 128)).T[:8]
        ss_send[layer, 0] = flat
        ss_send[layer, 1] = flat
        if layer == 0:
            pl.semaphore_wait(barrier, (p > 0).astype(jnp.int32) + (p < last).astype(jnp.int32) + phases)
        for way in range(2):
            at, side, hops, inward, _ = role(way)

            @pl.when((hops == 0) & (at != mid))
            def _():
                sq_copy(layer, way, side, inward).start()

        @pl.loop(0, chunks + final + LAG * mid)
        def _(t):
            @pl.when(t < chunks)
            def _():
                for copy in load_pair(layer, t):
                    copy.wait()
                w = jnp.concatenate(
                    [wg[layer, :, cols(t)].astype(jnp.bfloat16), wu[layer, :, cols(t)].astype(jnp.bfloat16)], axis=1)
                part[t] = jnp.dot(xs[...], w, preferred_element_type=jnp.float32)

            for way in range(2):
                at, side, hops, inward, outward = role(way)
                lo = way * half
                k = t - delay * side - LAG * hops
                inside = (k >= 0) & (k < chunks) & (at != mid)

                @pl.when(inside & (hops == 0))
                def _():
                    rs_send[layer, way, k] = part[k, lo:lo + half, :].astype(jnp.bfloat16)
                    rs_copy(layer, way, side, k, inward).start()

                @pl.when(inside & (hops > 0))
                def _():
                    @pl.when(k == 0)
                    def _():
                        sq_copy(layer, way, side, inward).wait_recv()
                        ss_send[layer, way] = ss_recv[layer, way, side] + ss_send[layer, way]
                        sq_copy(layer, way, side, inward).start()

                    rs_copy(layer, way, side, k, inward).wait_recv()
                    total = rs_recv[layer, way, side, k].astype(jnp.float32) + part[k, lo:lo + half, :]
                    rs_send[layer, way, k] = total.astype(jnp.bfloat16)
                    rs_copy(layer, way, side, k, inward).start()

                m = t - final

                @pl.when((m >= 0) & (m < chunks) & (at == mid))
                def _():
                    @pl.when(m == 0)
                    def _():
                        total = ss_send[layer, way]
                        for s in sides:
                            sq_copy(layer, way, s, inward).wait_recv()
                            total += ss_recv[layer, way, s]
                        column = jnp.broadcast_to(total[:1], (128, tok)).T
                        inv[way] = lax.rsqrt(column[lo:lo + half] / width + EPS)

                    total = part[m, lo:lo + half, :]
                    for s in sides:
                        rs_copy(layer, way, s, m, inward).wait_recv()
                        total += rs_recv[layer, way, s, m].astype(jnp.float32)
                    scale = inv[way]
                    gate = total[:, :CHUNK] * scale * gscale[cols(m)][None, :]
                    up = total[:, CHUNK:] * scale * uscale[cols(m)][None, :]
                    hidden = gate / (1.0 + jnp.exp(-gate)) * up
                    hid[layer, lo:lo + half, cols(m)] = hidden.astype(jnp.bfloat16)
                    for s in sides:
                        ag_copy(layer, way, s, m, place(way)[2 - s]).start()

                j = t - final - LAG * (at - mid) * (2 * side - 1)

                @pl.when((j >= 0) & (j < chunks) & (at != mid))
                def _():
                    ag_copy(layer, way, side, j, outward).wait_recv()

                    @pl.when(hops > 0)
                    def _():
                        ag_copy(layer, way, side, j, outward).start()

            if layer == 0:
                @pl.when(t == chunks)
                def _():
                    start_pairs(1)
                    load_down(1).start()

        load_down(layer).wait()
        down = jnp.dot(hid[layer], wd[layer].astype(jnp.bfloat16), preferred_element_type=jnp.float32)
        order = [(h, g) for g in range(PIECES) for h in range(2)]
        for h, g in order:
            lo = h * half + g * rows_of
            cb_send[layer, 0, h, g] = down[lo:lo + rows_of].astype(jnp.bfloat16)
            cb_copy(layer, 0, h, g).start()
        for phase in range(phases):
            for h, g in order:
                cb_copy(layer, phase, h, g).wait_recv()
                total = cb_send[layer, phase, h, g].astype(jnp.float32) + cb_recv[layer, phase, h, g].astype(jnp.float32)
                if phase < phases - 1:
                    cb_send[layer, phase + 1, h, g] = total.astype(jnp.bfloat16)
                    cb_copy(layer, phase + 1, h, g).start()
                else:
                    lo = h * half + g * rows_of
                    old = (tokens if layer == 0 else stream)[lo:lo + rows_of, :].astype(jnp.float32)
                    new = (RESID * old + total * dscale[...][None, :]).astype(jnp.bfloat16)
                    if layer == 0:
                        stream[lo:lo + rows_of, :] = new
                    else:
                        out[lo:lo + rows_of, :] = new

    for layer in range(2):
        for way in range(2):
            at, side, hops, inward, outward = role(way)

            @pl.when(at != mid)
            def _():
                sq_copy(layer, way, side, inward).wait_send()

                @pl.loop(0, chunks)
                def _(k):
                    rs_copy(layer, way, side, k, inward).wait_send()

            @pl.when((at != mid) & (hops > 0))
            def _():
                @pl.loop(0, chunks)
                def _(k):
                    ag_copy(layer, way, side, k, outward).wait_send()

            @pl.when(at == mid)
            def _():
                @pl.loop(0, chunks)
                def _(k):
                    for s in sides:
                        ag_copy(layer, way, s, k, outward).wait_send()

        for phase in range(phases):
            for h in range(2):
                for g in range(PIECES):
                    cb_copy(layer, phase, h, g).wait_send()


def solution(mesh):
    n_ra, n_cb = mesh.shape["ra"], mesh.shape["cb"]
    names = ("tokens", "g1", "wg1", "gs1", "wu1", "us1", "wd1", "ds1", "g2", "wg2", "gs2", "wu2", "us2", "wd2", "ds2")

    def body(*args):
        a = dict(zip(names, args))
        small = [a[k] for k in ("g1", "gs1", "us1", "ds1", "g2", "gs2", "us2", "ds2")]
        big = [a[k] for k in ("wg1", "wu1", "wd1", "wg2", "wu2", "wd2")]
        tok, dim = a["tokens"].shape
        ff = a["wg1"].shape[1]
        chunks, half, phases = ff // CHUNK, tok // 2, n_cb.bit_length() - 1
        f32, bf16, dma = jnp.float32, jnp.bfloat16, pltpu.SemaphoreType.DMA
        vmem = pl.BlockSpec(memory_space=pltpu.VMEM)
        piece = (2, phases, 2, PIECES)
        return pl.pallas_call(
            functools.partial(kernel, n_ra, n_cb, dim * n_ra),
            out_shape=jax.ShapeDtypeStruct((tok, dim), bf16),
            in_specs=[pl.BlockSpec(memory_space=pl.ANY)] * 15,
            out_specs=vmem,
            scratch_shapes=[
                pltpu.VMEM((tok, dim), bf16), *[pltpu.VMEM(v.shape, f32) for v in small],
                pltpu.VMEM((2, dim, ff), f32), pltpu.VMEM((2, dim, ff), f32), pltpu.VMEM((2, ff, dim), f32),
                pltpu.VMEM((chunks, tok, 2 * CHUNK), f32),
                pltpu.VMEM((2, 2, chunks, half, 2 * CHUNK), bf16),
                pltpu.VMEM((2, 2, 2, chunks, half, 2 * CHUNK), bf16),
                pltpu.VMEM((2, tok, ff), bf16),
                pltpu.VMEM((2, 2, 8, tok), f32), pltpu.VMEM((2, 2, 2, 8, tok), f32),
                pltpu.VMEM((2, half, 128), f32),
                pltpu.VMEM((tok, dim), bf16), pltpu.VMEM((tok, dim), bf16),
                pltpu.VMEM(piece + (half // PIECES, dim), bf16), pltpu.VMEM(piece + (half // PIECES, dim), bf16),
                dma((9,)), dma((2, chunks)), dma((2, chunks)), dma((2,)),
                dma((2, 2, chunks)), dma((2, 2, 2, chunks)), dma((2, 2, 2, chunks)), dma((2, 2, chunks)),
                dma((2, 2)), dma((2, 2, 2)), dma(piece), dma(piece),
            ],
            compiler_params=pltpu.CompilerParams(
                collective_id=0, has_side_effects=True, vmem_limit_bytes=56 * 1024 * 1024),
        )(a["tokens"], *small, *big)

    in_specs = (
        P("dp", "ra"),
        P("ra"), P("ra", "cb"), P("cb"), P("ra", "cb"), P("cb"), P("cb", "ra"), P("ra"),
        P("ra"), P("ra", "cb"), P("cb"), P("ra", "cb"), P("cb"), P("cb", "ra"), P("ra"),
    )
    return jax.shard_map(body, mesh=mesh, in_specs=in_specs, out_specs=P("dp", "ra"), check_vma=False)
```

time: 83.1 us -> 68.8 us (0.83)
  Pallas kernels: 76 us -> 67.1 us
  local copies, waits for them, and re-layouts: 6.73 us -> 1.57 us
    pallas_call x1, Pallas kernels: 76 us -> 67.1 us  [body(): pl.pallas_call(functools.partial(kernel, n_ra, n_cb, dim * n_ra), out_sha...]
    reshape x4 -> x0, local copies, waits for them, and re-layouts: 5.16 us -> none  [body(): a[k].reshape(1, -1)]
where the time goes in v2:
time: 68.8 us; the launch traced here: 68.7 us
  Pallas kernels  67.1 us (98%)
  local copies, waits for them, and re-layouts  1.57 us (2%)
    pallas_call x1, Pallas kernels, body(): pl.pallas_call(functools.partial(kernel, n_ra, n_cb, dim * n_ra), out_sha...  67.1 us
    unnamed x1, local copies, waits for them, and re-layouts  1.57 us

profile of v2, /device:TPU:0, one launch (start us, length us, event | category | flops | bytes accessed | tf_op | source)
XLA Modules:
  0.0 68.7 jit_solution(5359623116893435771)
XLA Ops:
  0.0 67.1 %shard_map.145 = bf16[128,512]{1,0:T(8,128)(2,1)} custom-call(bf16[128,512]{1,0:T(8,128)(2,1)} %tokens_in.1, f32[512]{0:T(512)} %gain1_in.1, f32[1408]{0:T(1024)} %gs1_in.1, f32[1408]{0:T(1024)} %us1_in.1, f32[512]{0:T(512)} %ds1_in.1, f32[512]{0:T(512)} %gain2_in.1, f32[1408]{0:T(1024)} %gs2_in.1, f32[1408]{0:T(1024)} %us2_in.1, f32[512]{0:T(512)} %ds2_in.1, ...), custom_call_target="tpu_custom_call" | custom-call | tf_op jit(solution)/shard_map/pallas_call | solution.py:287
  67.1 1.6 %copy.17 = bf16[128,512]{1,0:T(8,128)(2,1)} copy(bf16[128,512]{1,0:T(8,128)(2,1)} %shard_map.145) | data formatting | bytes 262144

commit v3 on v2

--- a/solution.py
+++ b/solution.py
@@ -1,4 +1,5 @@
 import functools
+import itertools
 
 import jax
 import jax.numpy as jnp
@@ -12,6 +13,7 @@
 MESH = pl.DeviceIdType.MESH
 CHUNK = 128
 LAG = 5
+FAR = 4
 PIECES = 2
 
 
@@ -81,16 +83,20 @@
         pl.semaphore_signal(barrier, inc=1, device_id={"cb": partner(1 << b)}, device_id_type=MESH)
 
     mid = n_ra // 2
-    delay = chunks
-    final = max(LAG * mid, delay + LAG * (last - mid)) if last > mid else LAG * mid
-    sides = range(2 if last > mid else 1)
+    both = range(2 if last > mid else 1)
+    near_delay = chunks - FAR
+    groups = (
+        (last, 0, FAR, range(1), 0, LAG * last),
+        (mid, FAR, chunks, both, near_delay, max(LAG * mid, near_delay + LAG * (last - mid))),
+    )
+    ticks = max(end + final + LAG * owner for owner, _, end, _, _, final in groups)
 
     def place(way):
         return (p, p + 1, p - 1) if way == 0 else (last - p, p - 1, p + 1)
 
-    def role(way):
+    def role(way, owner):
         at, ahead, behind = place(way)
-        side = (at > mid).astype(jnp.int32)
+        side = (at > owner).astype(jnp.int32)
         hops = at + side * (last - 2 * at)
         inward = ahead + side * (behind - ahead)
         return at, side, hops, inward, ahead + behind - inward
@@ -101,10 +107,10 @@
             send_sem=rs_ss.at[layer, way, k], recv_sem=rs_rs.at[layer, way, side, k],
             device_id={"ra": to}, device_id_type=MESH)
 
-    def sq_copy(layer, way, side, to):
+    def sq_copy(layer, way, group, side, to):
         return pltpu.make_async_remote_copy(
-            src_ref=ss_send.at[layer, way], dst_ref=ss_recv.at[layer, way, side],
-            send_sem=sq_ss.at[layer, way], recv_sem=sq_rs.at[layer, way, side],
+            src_ref=ss_send.at[layer, way, group], dst_ref=ss_recv.at[layer, way, group, side],
+            send_sem=sq_ss.at[layer, way, group], recv_sem=sq_rs.at[layer, way, group, side],
             device_id={"ra": to}, device_id_type=MESH)
 
     def ag_copy(layer, way, side, k, to):
@@ -130,18 +136,20 @@
         xs[...] = (values * gain[...][None, :]).astype(jnp.bfloat16)
         sums = jnp.sum(values * values, axis=-1, keepdims=True)
         flat = jnp.broadcast_to(sums, (tok, 128)).T[:8]
-        ss_send[layer, 0] = flat
-        ss_send[layer, 1] = flat
+        for way in range(2):
+            for group in range(2):
+                ss_send[layer, way, group] = flat
         if layer == 0:
             pl.semaphore_wait(barrier, (p > 0).astype(jnp.int32) + (p < last).astype(jnp.int32) + phases)
         for way in range(2):
-            at, side, hops, inward, _ = role(way)
-
-            @pl.when((hops == 0) & (at != mid))
-            def _():
-                sq_copy(layer, way, side, inward).start()
-
-        @pl.loop(0, chunks + final + LAG * mid)
+            for group, (owner, *_) in enumerate(groups):
+                at, side, hops, inward, _ = role(way, owner)
+
+                @pl.when((hops == 0) & (at != owner))
+                def _():
+                    sq_copy(layer, way, group, side, inward).start()
+
+        @pl.loop(0, ticks)
         def _(t):
             @pl.when(t < chunks)
             def _():
@@ -151,11 +159,11 @@
                     [wg[layer, :, cols(t)].astype(jnp.bfloat16), wu[layer, :, cols(t)].astype(jnp.bfloat16)], axis=1)
                 part[t] = jnp.dot(xs[...], w, preferred_element_type=jnp.float32)
 
-            for way in range(2):
-                at, side, hops, inward, outward = role(way)
+            for way, (group, (owner, first, end, sides, delay, final)) in itertools.product(range(2), enumerate(groups)):
+                at, side, hops, inward, outward = role(way, owner)
                 lo = way * half
                 k = t - delay * side - LAG * hops
-                inside = (k >= 0) & (k < chunks) & (at != mid)
+                inside = (k >= first) & (k < end) & (at != owner)
 
                 @pl.when(inside & (hops == 0))
                 def _():
@@ -164,11 +172,11 @@
 
                 @pl.when(inside & (hops > 0))
                 def _():
-                    @pl.when(k == 0)
+                    @pl.when(k == first)
                     def _():
-                        sq_copy(layer, way, side, inward).wait_recv()
-                        ss_send[layer, way] = ss_recv[layer, way, side] + ss_send[layer, way]
-                        sq_copy(layer, way, side, inward).start()
+                        sq_copy(layer, way, group, side, inward).wait_recv()
+                        ss_send[layer, way, group] = ss_recv[layer, way, group, side] + ss_send[layer, way, group]
+                        sq_copy(layer, way, group, side, inward).start()
 
                     rs_copy(layer, way, side, k, inward).wait_recv()
                     total = rs_recv[layer, way, side, k].astype(jnp.float32) + part[k, lo:lo + half, :]
@@ -177,14 +185,14 @@
 
                 m = t - final
 
-                @pl.when((m >= 0) & (m < chunks) & (at == mid))
-                def _():
-                    @pl.when(m == 0)
+                @pl.when((m >= first) & (m < end) & (at == owner))
+                def _():
+                    @pl.when(m == first)
                     def _():
-                        total = ss_send[layer, way]
+                        total = ss_send[layer, way, group]
                         for s in sides:
-                            sq_copy(layer, way, s, inward).wait_recv()
-                            total += ss_recv[layer, way, s]
+                            sq_copy(layer, way, group, s, inward).wait_recv()
+                            total += ss_recv[layer, way, group, s]
                         column = jnp.broadcast_to(total[:1], (128, tok)).T
                         inv[way] = lax.rsqrt(column[lo:lo + half] / width + EPS)
 
@@ -200,9 +208,9 @@
                     for s in sides:
                         ag_copy(layer, way, s, m, place(way)[2 - s]).start()
 
-                j = t - final - LAG * (at - mid) * (2 * side - 1)
-
-                @pl.when((j >= 0) & (j < chunks) & (at != mid))
+                j = t - final - LAG * (at - owner) * (2 * side - 1)
+
+                @pl.when((j >= first) & (j < end) & (at != owner))
                 def _():
                     ag_copy(layer, way, side, j, outward).wait_recv()
 
@@ -240,26 +248,26 @@
                         out[lo:lo + rows_of, :] = new
 
     for layer in range(2):
-        for way in range(2):
-            at, side, hops, inward, outward = role(way)
-
-            @pl.when(at != mid)
+        for way, (group, (owner, first, end, sides, _, _)) in itertools.product(range(2), enumerate(groups)):
+            at, side, hops, inward, outward = role(way, owner)
+
+            @pl.when(at != owner)
             def _():
-                sq_copy(layer, way, side, inward).wait_send()
-
-                @pl.loop(0, chunks)
+                sq_copy(layer, way, group, side, inward).wait_send()
+
+                @pl.loop(first, end)
                 def _(k):
                     rs_copy(layer, way, side, k, inward).wait_send()
 
-            @pl.when((at != mid) & (hops > 0))
+            @pl.when((at != owner) & (hops > 0))
             def _():
-                @pl.loop(0, chunks)
+                @pl.loop(first, end)
                 def _(k):
                     ag_copy(layer, way, side, k, outward).wait_send()
 
-            @pl.when(at == mid)
+            @pl.when(at == owner)
             def _():
-                @pl.loop(0, chunks)
+                @pl.loop(first, end)
                 def _(k):
                     for s in sides:
                         ag_copy(layer, way, s, k, outward).wait_send()
@@ -296,13 +304,13 @@
                 pltpu.VMEM((2, 2, chunks, half, 2 * CHUNK), bf16),
                 pltpu.VMEM((2, 2, 2, chunks, half, 2 * CHUNK), bf16),
                 pltpu.VMEM((2, tok, ff), bf16),
-                pltpu.VMEM((2, 2, 8, tok), f32), pltpu.VMEM((2, 2, 2, 8, tok), f32),
+                pltpu.VMEM((2, 2, 2, 8, tok), f32), pltpu.VMEM((2, 2, 2, 2, 8, tok), f32),
                 pltpu.VMEM((2, half, 128), f32),
                 pltpu.VMEM((tok, dim), bf16), pltpu.VMEM((tok, dim), bf16),
                 pltpu.VMEM(piece + (half // PIECES, dim), bf16), pltpu.VMEM(piece + (half // PIECES, dim), bf16),
                 dma((9,)), dma((2, chunks)), dma((2, chunks)), dma((2,)),
                 dma((2, 2, chunks)), dma((2, 2, 2, chunks)), dma((2, 2, 2, chunks)), dma((2, 2, chunks)),
-                dma((2, 2)), dma((2, 2, 2)), dma(piece), dma(piece),
+                dma((2, 2, 2)), dma((2, 2, 2, 2)), dma(piece), dma(piece),
             ],
             compiler_params=pltpu.CompilerParams(
                 collective_id=0, has_side_effects=True, vmem_limit_bytes=56 * 1024 * 1024),

time: 68.8 us -> 66.6 us (0.968)
  Pallas kernels: 67.1 us -> 64.8 us
    pallas_call x1, Pallas kernels: 67.1 us -> 64.8 us  [body(): pl.pallas_call(functools.partial(kernel, n_ra, n_cb, dim * n_ra), out_sha...]
where the time goes in v3:
time: 66.6 us; the launch traced here: 66.4 us
  Pallas kernels  64.8 us (97%)
  local copies, waits for them, and re-layouts  1.57 us (2%)
    pallas_call x1, Pallas kernels, body(): pl.pallas_call(functools.partial(kernel, n_ra, n_cb, dim * n_ra), out_sha...  64.8 us
    unnamed x1, local copies, waits for them, and re-layouts  1.57 us

profile of v3, /device:TPU:0, one launch (start us, length us, event | category | flops | bytes accessed | tf_op | source)
XLA Modules:
  0.0 66.4 jit_solution(404289324483871487)
XLA Ops:
  0.0 64.8 %shard_map.145 = bf16[128,512]{1,0:T(8,128)(2,1)} custom-call(bf16[128,512]{1,0:T(8,128)(2,1)} %tokens_in.1, f32[512]{0:T(512)} %gain1_in.1, f32[1408]{0:T(1024)} %gs1_in.1, f32[1408]{0:T(1024)} %us1_in.1, f32[512]{0:T(512)} %ds1_in.1, f32[512]{0:T(512)} %gain2_in.1, f32[1408]{0:T(1024)} %gs2_in.1, f32[1408]{0:T(1024)} %us2_in.1, f32[512]{0:T(512)} %ds2_in.1, ...), custom_call_target="tpu_custom_call" | custom-call | tf_op jit(solution)/shard_map/pallas_call | solution.py:295
  64.9 1.6 %copy.17 = bf16[128,512]{1,0:T(8,128)(2,1)} copy(bf16[128,512]{1,0:T(8,128)(2,1)} %shard_map.145) | data formatting | bytes 262144
